TPU v7x, 32 devices: a whole 2x2x4 slice. The times are simulated.
32 devices in a mesh: sp: 8 (over z, x), dp: 4 (over y, core).
Axes of the slice: x: 2, y: 2, z: 4, core: 2. Of those that a mesh axis runs over, the one named last changes fastest.
Arguments:
- gate_in: bfloat16 [4, 4096, 1024], P('dp', 'sp'), may hold values from -6 to 6
- value_in: bfloat16 [4, 4096, 1024], P('dp', 'sp'), may hold values from -6 to 6
- segments: int32 [4, 4096], P('dp', 'sp'), may hold values from 0 to 1, never falling along the last dimension, each value on 1 to 3072 neighbouring positions
- value_gain: bfloat16 [1024], P('sp'), may hold values from 0.099609375 to 1.8984375
- mixing: bfloat16 [8, 1024, 1024], P('sp', 'dp'), may hold values from -0.1875 to 0.1875
- mixing_bias: bfloat16 [8, 1024], P('sp'), may hold values from 0.099609375 to 1.8984375
Outputs:
- gated: bfloat16 [4, 4096, 1024], P('dp', 'sp')
Inputs may be any that keep to these rules, and one draw needn't show every extreme that they name: `segments`: within each sequence the numbers never fall, every number 0 to 1 occurs, a document spans at most 3072 positions and some document spans exactly that.
All inputs are finite; a program needn't handle non-finite values.
Results may differ from a plain program's by a relative error of at most 0.0054.
Values may be sent and summed in bfloat16 or wider, within the bound.
A program may use at most 128 MiB of HBM per device.

v0:
```python
import jax
import jax.numpy as jnp
from jax import lax
from jax.sharding import PartitionSpec as P

HEAD_DIM = 128


epsilon = 1e-06


def head_norm(values, gain_f, head_dim):
    shaped = values.reshape(values.shape[:-1] + (values.shape[-1] // head_dim, head_dim))
    scaled = shaped * lax.rsqrt(jnp.mean(shaped * shaped, axis=-1, keepdims=True) + epsilon)
    return (scaled.reshape(values.shape) * gain_f).astype(jnp.bfloat16)


def per_device(gate_in, value_in, segments, value_gain, mixing, mixing_bias):
    sp_count = lax.axis_size("sp")
    sequences = value_in.shape[0]
    tokens = value_in.shape[1]
    length = tokens * sp_count
    block_len = mixing.shape[2]
    heads_here = mixing.shape[0]
    head_dim = HEAD_DIM
    id_tile = jnp.broadcast_to(
        segments.astype(jnp.bfloat16)[:, :, None], (sequences, tokens, sp_count)
    )
    value_heads, id_heads = (
        lax.all_to_all(value_in, "sp", split_axis=2, concat_axis=1, tiled=True),
        lax.all_to_all(id_tile, "sp", split_axis=2, concat_axis=1, tiled=True),
    )
    gain_f = value_gain.astype(jnp.float32)
    normed = head_norm(jax.nn.gelu(value_heads.astype(jnp.float32)), gain_f, head_dim)
    blocks = sequences * length // block_len
    value_blocks = normed.reshape(blocks, block_len, heads_here, head_dim)
    id_blocks = id_heads.reshape(blocks, block_len)
    bias_f = mixing_bias.astype(jnp.float32)
    nothing = jnp.zeros((), jnp.bfloat16)
    shard_piece = lax.all_gather(mixing, "dp", axis=1, tiled=True)
    bias_rows = jnp.transpose(bias_f)[:, :, None]

    def one_block(pair_item):
        block_values, block_ids = pair_item
        same_doc = block_ids[:, None] == block_ids[None, :]
        masked = jnp.where(same_doc[None, :, :], shard_piece, nothing)
        summed = jnp.einsum(
            "hts,shd->thd", masked, block_values, preferred_element_type=jnp.float32
        )
        return (summed + bias_rows).astype(jnp.bfloat16)

    mixed = lax.map(one_block, (value_blocks, id_blocks))
    mixed = mixed.reshape(sequences, length, heads_here * head_dim)
    returned = lax.all_to_all(mixed, "sp", split_axis=1, concat_axis=2, tiled=True)
    return (jax.nn.gelu(gate_in.astype(jnp.float32)) * returned.astype(jnp.float32)).astype(
        jnp.bfloat16
    )


def solution(mesh):
    return jax.shard_map(
        per_device,
        mesh=mesh,
        in_specs=(
            P("dp", "sp", None),
            P("dp", "sp", None),
            P("dp", "sp"),
            P("sp"),
            P("sp", "dp", None),
            P("sp", None),
        ),
        out_specs=P("dp", "sp", None),
        check_vma=False,
    )
```

profile of v0, /device:TPU:0, one launch (start us, length us, event | category | flops | bytes accessed | tf_op | source)
XLA Modules:
  0.0 162.7 jit_solution(6695371021300023633)
XLA Ops:
  6.5 0.7 all-gather.2.cloned.1.call-update
  7.3 0.7 convert_reduce_fusion
  8.0 0.5 broadcast.193
  8.5 0.6 reduce.7
  9.0 0.6 reshape.283
  9.7 7.3 %all-to-all-start.1 = ((bf16[8,2,256]{2,1,0:T(2,128)(2,1)}), bf16[8,2,256]{2,1,0:T(2,128)(2,1)S(1)}, u32[]{:S(2)}, u32[]{:S(2)}) async-start(bf16[8,2,256]{2,1,0:T(2,128)(2,1)} %reshape.283), calls=%async_computation.1 | async-start | bytes 16384 | tf_op jit(solution)/shard_map/all_to_all | solution.py:31
  16.9 4.7 %copy.44 = bf16[1,512,1024]{1,0,2:T(2,128)(2,1)S(1)} copy(bf16[1,512,1024]{2,1,0:T(8,128)(2,1)} %param.9) | data formatting | bytes 2097152 | tf_op args[1]
  21.6 6.9 %reduce.6 = bf16[1024,512]{1,0:T(8,128)(2,1)S(1)} reduce(bf16[1024,1,512]{2,1,0:T(2,128)(2,1)S(1)} %bitcast.83, bf16[]{:T(256)} %broadcast.193), dimensions={1}, to_apply=%bitcast.59.reduce_sub_computation | reduce | bytes 2097154
  28.6 1.6 reshape.281
  30.2 6.0 %all-to-all-start = ((bf16[8,2,32768]{2,1,0:T(2,128)(2,1)}), bf16[8,2,32768]{2,1,0:T(2,128)(2,1)S(1)}, u32[]{:S(2)}, u32[]{:S(2)}) async-start(bf16[8,2,32768]{2,1,0:T(2,128)(2,1)} %reshape.281), calls=%async_computation | async-start | bytes 2097152 | tf_op jit(solution)/shard_map/all_to_all | solution.py:30
  36.3 25.3 %all-to-all-done = bf16[8,2,32768]{2,1,0:T(2,128)(2,1)S(1)} async-done(((bf16[8,2,32768]{2,1,0:T(2,128)(2,1)}), bf16[8,2,32768]{2,1,0:T(2,128)(2,1)S(1)}, u32[]{:S(2)}, u32[]{:S(2)}) %all-to-all-start) | async-done | bytes 1048608 | tf_op jit(solution)/shard_map/all_to_all | solution.py:30
  61.6 1.0 reshape.282
  62.6 0.3 copy.45
  62.9 0.5 copy.46
  63.5 0.8 fusion.47
  64.4 1.7 %fusion.31 = bf16[4,1024,1,128]{3,1,2,0:T(8,128)(2,1)} fusion(f32[4,1024,1,128]{3,1,2,0:T(8,128)S(1)} %bitcast.79, f32[128]{0:T(128)S(1)} %convert_element_type.89, f32[4,1024]{1,0:T(4,128)S(1)} %rsqrt.12), kind=kLoop, calls=%fused_computation.31 | loop fusion | flops 5767168 | bytes 3162624 | tf_op jit(solution)/shard_map/convert_element_type | solution.py:15
  66.0 11.5 %while.10 = (s32[]{:T(128)}, bf16[4,1024,1,128]{3,1,0,2:T(8,128)(2,1)S(1)}, bf16[4,1024,1,128]{3,1,2,0:T(8,128)(2,1)}, bf16[4,1024]{1,0:T(4,128)(2,1)S(1)}, bf16...) while((s32[]{:T(128)}, bf16[4,1024,1,128]{3,1,0,2:T(8,128)(2,1)S(1)}, ...), condition=%wide.region_2.3_spmd, body=%wide.region_1.2_spmd.sunk | while | flops 270794752 | bytes 3682901 | solution.py:52
  66.1 2.6 %fusion.53 = bf16[1,1024,1,128]{1,3,2,0:T(8,128)(2,1)S(1)} fusion(bf16[1,1024,1024]{2,1,0:T(8,128)(2,1)} %get-tuple-element.105, bf16[1024]{0:T(1024)(128)(2,1)S(1)} %dynamic-slice_reduce_fusion.2, f32[1024]{0:T(1024)S(1)} %bitcast.89, bf16[4,1024,1,128]{3,1,2,0:T(8,128)(2,1)} %get-tuple-element.103, s32[]{:T(128)} %get-tuple-element.94), kind=kOutput, calls=%fused_computation.6.clone.1 | convolution fusion | flops 270794752 | bytes 2630144 | tf_op jit(solution)/shard_map/while/body/eval_jaxpr/hts,shd->thd/dot_general | solution.py:47
  69.0 2.6 %fusion.53 = bf16[1,1024,1,128]{1,3,2,0:T(8,128)(2,1)S(1)} fusion(bf16[1,1024,1024]{2,1,0:T(8,128)(2,1)} %get-tuple-element.105, bf16[1024]{0:T(1024)(128)(2,1)S(1)} %dynamic-slice_reduce_fusion.2, f32[1024]{0:T(1024)S(1)} %bitcast.89, bf16[4,1024,1,128]{3,1,2,0:T(8,128)(2,1)} %get-tuple-element.103, s32[]{:T(128)} %get-tuple-element.94), kind=kOutput, calls=%fused_computation.6.clone.1 | convolution fusion | flops 270794752 | bytes 2630144 | tf_op jit(solution)/shard_map/while/body/eval_jaxpr/hts,shd->thd/dot_general | solution.py:47
  71.8 2.6 %fusion.53 = bf16[1,1024,1,128]{1,3,2,0:T(8,128)(2,1)S(1)} fusion(bf16[1,1024,1024]{2,1,0:T(8,128)(2,1)} %get-tuple-element.105, bf16[1024]{0:T(1024)(128)(2,1)S(1)} %dynamic-slice_reduce_fusion.2, f32[1024]{0:T(1024)S(1)} %bitcast.89, bf16[4,1024,1,128]{3,1,2,0:T(8,128)(2,1)} %get-tuple-element.103, s32[]{:T(128)} %get-tuple-element.94), kind=kOutput, calls=%fused_computation.6.clone.1 | convolution fusion | flops 270794752 | bytes 2630144 | tf_op jit(solution)/shard_map/while/body/eval_jaxpr/hts,shd->thd/dot_general | solution.py:47
  74.7 2.6 %fusion.53 = bf16[1,1024,1,128]{1,3,2,0:T(8,128)(2,1)S(1)} fusion(bf16[1,1024,1024]{2,1,0:T(8,128)(2,1)} %get-tuple-element.105, bf16[1024]{0:T(1024)(128)(2,1)S(1)} %dynamic-slice_reduce_fusion.2, f32[1024]{0:T(1024)S(1)} %bitcast.89, bf16[4,1024,1,128]{3,1,2,0:T(8,128)(2,1)} %get-tuple-element.103, s32[]{:T(128)} %get-tuple-element.94), kind=kOutput, calls=%fused_computation.6.clone.1 | convolution fusion | flops 270794752 | bytes 2630144 | tf_op jit(solution)/shard_map/while/body/eval_jaxpr/hts,shd->thd/dot_general | solution.py:47
  77.6 16.7 %copy.63 = bf16[1,4096,128]{2,0,1:T(2,128)(2,1)S(1)} copy(bf16[1,4096,128]{2,1,0:T(8,128)(2,1)S(1)} %bitcast.86) | data formatting | bytes 2097152 | tf_op jit(solution)/shard_map/reshape | solution.py:53
  94.3 22.3 %reduce.8 = bf16[4096,128]{1,0:T(8,128)(2,1)S(1)} reduce(bf16[4096,1,128]{2,1,0:T(2,128)(2,1)S(1)} %bitcast.82, bf16[]{:T(256)} %broadcast.193), dimensions={1}, to_apply=%bitcast.68.reduce_sub_computation | reduce | bytes 2097154
  116.6 1.1 reshape.285
  117.7 3.6 %all-to-all-start.2 = ((bf16[8,2,32768]{2,1,0:T(2,128)(2,1)}), bf16[8,2,32768]{2,1,0:T(2,128)(2,1)S(1)}, u32[]{:S(2)}, u32[]{:S(2)}) async-start(bf16[8,2,32768]{2,1,0:T(2,128)(2,1)} %reshape.285), calls=%async_computation.2 | async-start | bytes 2097152 | tf_op jit(solution)/shard_map/all_to_all | solution.py:54
  121.3 1.3 copy.43
  122.6 24.4 %all-to-all-done.2 = bf16[8,2,32768]{2,1,0:T(2,128)(2,1)S(1)} async-done(((bf16[8,2,32768]{2,1,0:T(2,128)(2,1)}), bf16[8,2,32768]{2,1,0:T(2,128)(2,1)S(1)}, u32[]{:S(2)}, u32[]{:S(2)}) %all-to-all-start.2) | async-done | bytes 1048608 | tf_op jit(solution)/shard_map/all_to_all | solution.py:54
  147.1 1.0 reshape.286
  148.3 1.5 convert_bitcast_fusion
  149.8 2.0 %copy.55 = f32[1,512,8,128]{1,3,2,0:T(8,128)S(1)} copy(f32[1,512,8,128]{3,1,2,0:T(8,128)} %convert_bitcast_fusion) | data formatting | bytes 4194304 | tf_op jit(solution)/shard_map/convert_element_type | solution.py:55
  151.8 1.8 %fusion.46 = bf16[1,512,1024]{1,2,0:T(8,128)(2,1)} fusion(bf16[1,512,1024]{1,2,0:T(8,128)(2,1)S(1)} %copy-done, f32[1,512,8,128]{1,3,2,0:T(8,128)S(1)} %copy.55), kind=kLoop, calls=%fused_computation.46 | loop fusion | flops 5767168 | bytes 4194304 | tf_op jit(solution)/shard_map/convert_element_type | solution.py:55
  153.6 2.3 %copy.56 = bf16[1,512,1024]{2,1,0:T(8,128)(2,1)} copy(bf16[1,512,1024]{1,2,0:T(8,128)(2,1)} %fusion.46) | data formatting | bytes 2097152 | tf_op jit(solution)/shard_map/convert_element_type | solution.py:55
  (35 shorter events, 1.2 us)
Async XLA Ops:
  6.5 59.5 %all-gather.2.cloned.1.call-start = ((), (), s32[]{:S(2)}) async-start(), calls=%async_computation.3 | async-start | bytes 2621440 | tf_op jit(solution)/shard_map/all_gather | solution.py:40
  9.7 20.5 %all-to-all-start.1 = ((bf16[8,2,256]{2,1,0:T(2,128)(2,1)}), bf16[8,2,256]{2,1,0:T(2,128)(2,1)S(1)}, u32[]{:S(2)}, u32[]{:S(2)}) async-start(bf16[8,2,256]{2,1,0:T(2,128)(2,1)} %reshape.283), calls=%async_computation.1 | async-start | bytes 16384 | tf_op jit(solution)/shard_map/all_to_all | solution.py:31
  28.6 7.6 %copy-start.4 = (bf16[128]{0:T(256)(128)(2,1)S(1)}, bf16[128]{0:T(256)(128)(2,1)}, u32[]{:S(2)}) copy-start(bf16[128]{0:T(256)(128)(2,1)} %param.11) | copy-start | bytes 772
  28.6 7.6 %copy-start.3 = (bf16[1,1024]{1,0:T(2,128)(2,1)S(1)}, bf16[1,1024]{1,0:T(2,128)(2,1)}, u32[]{:S(2)}) copy-start(bf16[1,1024]{1,0:T(2,128)(2,1)} %param.13) | copy-start | bytes 6148
  30.2 31.4 %all-to-all-start = ((bf16[8,2,32768]{2,1,0:T(2,128)(2,1)}), bf16[8,2,32768]{2,1,0:T(2,128)(2,1)S(1)}, u32[]{:S(2)}, u32[]{:S(2)}) async-start(bf16[8,2,32768]{2,1,0:T(2,128)(2,1)} %reshape.281), calls=%async_computation | async-start | bytes 2097152 | tf_op jit(solution)/shard_map/all_to_all | solution.py:30
  64.3 1.7 %copy-start.1 = (bf16[4,1024,1,128]{3,1,0,2:T(8,128)(2,1)S(1)}, bf16[4,1024,1,128]{3,1,0,2:T(8,128)(2,1)}, u32[]{:S(2)}) copy-start(bf16[4,1024,1,128]{3,1,0,2:T(8,128)(2,1)} %custom-call) | copy-start | bytes 3145732
  116.6 4.7 %copy-start.2 = (bf16[1,512,1024]{2,1,0:T(8,128)(2,1)S(1)}, bf16[1,512,1024]{2,1,0:T(8,128)(2,1)}, u32[]{:S(2)}) copy-start(bf16[1,512,1024]{2,1,0:T(8,128)(2,1)} %param.8) | copy-start | bytes 3145732
  117.7 29.3 %all-to-all-start.2 = ((bf16[8,2,32768]{2,1,0:T(2,128)(2,1)}), bf16[8,2,32768]{2,1,0:T(2,128)(2,1)S(1)}, u32[]{:S(2)}, u32[]{:S(2)}) async-start(bf16[8,2,32768]{2,1,0:T(2,128)(2,1)} %reshape.285), calls=%async_computation.2 | async-start | bytes 2097152 | tf_op jit(solution)/shard_map/all_to_all | solution.py:54
  149.8 2.0 %copy-start = (bf16[1,512,1024]{1,2,0:T(8,128)(2,1)S(1)}, bf16[1,512,1024]{1,2,0:T(8,128)(2,1)}, u32[]{:S(2)}) copy-start(bf16[1,512,1024]{1,2,0:T(8,128)(2,1)} %copy.43) | copy-start | bytes 3145732
Sparse Core Ops, SparseCore 0:
  8.9 25.2 all-gather.1
where the time goes:
time: 163 us
  waiting for transfers between devices  50.5 us (31%)
  other arithmetic  36.3 us (22%)
  local copies, waits for them, and re-layouts  34.9 us (21%)
  starting transfers between devices  16.8 us (10%)
  between operations  13.6 us (8%)
  matrix products  10.4 us (6%)
    unnamed x3, other arithmetic  29.8 us
    all_to_all x1, waiting for transfers between devices, per_device(): lax.all_to_all(value_in, 'sp', split_axis=2, concat_axis=1, tiled=True)  25.3 us
    all_to_all x1, waiting for transfers between devices, per_device(): lax.all_to_all(mixed, 'sp', split_axis=1, concat_axis=2, tiled=True)  24.4 us
    reshape x1, local copies, waits for them, and re-layouts, per_device(): mixed = mixed.reshape(sequences, length, heads_here * head_dim)  16.7 us
    unnamed x21, local copies, waits for them, and re-layouts  11.9 us
    dot_general x4, matrix products, one_block(): jnp.einsum('hts,shd->thd', masked, block_values, preferred_element_type=j...  10.4 us
    all_to_all x1, starting transfers between devices, per_device(): lax.all_to_all(id_tile, 'sp', split_axis=2, concat_axis=1, tiled=True)  7.28 us
    all_to_all x1, starting transfers between devices, per_device(): lax.all_to_all(value_in, 'sp', split_axis=2, concat_axis=1, tiled=True)  5.99 us
  transfers between devices with their start and end apart: 4, of which 2 were waited for; matrix products, arithmetic and copies ran while one was open for 13% of the time, Pallas kernels for 0%

commit v1 on v0

v1 whole, which is shorter than its diff:
```python
import functools

import jax
import jax.numpy as jnp
from jax import lax
from jax.experimental import pallas as pl
from jax.experimental.pallas import tpu as pltpu
from jax.sharding import PartitionSpec as P

HEAD_DIM = 128
CORES = 2
LANES = 128
ROW_STEP = 256
MESH = pl.DeviceIdType.MESH

epsilon = 1e-06


def flip(a, b, count):
    total, bit = 0, 1
    while bit < count:
        total = total + ((a // bit + b // bit) % 2) * bit
        bit *= 2
    return total


def gelu(x):
    return jax.nn.gelu(x, approximate=True)


def to_column(row):
    parts = []
    for at in range(0, row.shape[1], LANES):
        piece = jnp.broadcast_to(row[:, at : at + LANES], (LANES, LANES))
        parts.append(piece.T)
    return jnp.concatenate(parts, axis=0)


def kernel(
    sp, dp, value_ref, ids_ref, gain_ref, mixing_ref, bias_ref, gate_ref, out_ref,
    vals, ids, mix, res, ret, bias_col, normed, ids_col,
    v_send, v_recv, i_send, i_recv, r_send, r_recv, m_send, m_recv, m_fwd, own_sem,
):
    s, d = lax.axis_index("sp"), lax.axis_index("dp")
    tokens = value_ref.shape[0]
    block_len = mix.shape[0]
    per = block_len // tokens
    blocks = sp // per
    rows = mixing_ref.shape[0]
    planes = dp // CORES
    half = s % per
    partner = d + 1 - 2 * (d % CORES)
    plane, core = d // CORES, d % CORES

    def across(step):
        return ((plane + step) % planes) * CORES + core

    barrier = pltpu.get_barrier_semaphore()
    for k in range(1, sp):
        pl.semaphore_signal(barrier, inc=1, device_id={"sp": flip(s, k, sp)}, device_id_type=MESH)
    pl.semaphore_signal(barrier, inc=1, device_id={"dp": partner}, device_id_type=MESH)
    for step in range(1, planes):
        pl.semaphore_signal(barrier, inc=1, device_id={"dp": across(step)}, device_id_type=MESH)
    pl.semaphore_wait(barrier, sp - 1 + planes)

    def chunk(of):
        return mix.at[pl.ds(pl.multiple_of(of * rows, rows), rows)]

    def mix_copy(src, origin, target, sem):
        return pltpu.make_async_remote_copy(
            src_ref=src, dst_ref=chunk(origin), send_sem=sem, recv_sem=m_recv.at[origin],
            device_id={"dp": target}, device_id_type=MESH,
        )

    def value_copy(k, end):
        target = flip(s, k, sp)
        return pltpu.make_async_remote_copy(
            src_ref=value_ref.at[:, pl.ds(pl.multiple_of(target * HEAD_DIM, HEAD_DIM), HEAD_DIM)],
            dst_ref=vals.at[k // per, pl.ds(pl.multiple_of(end * tokens, tokens), tokens)],
            send_sem=v_send.at[k], recv_sem=v_recv.at[k],
            device_id={"sp": target}, device_id_type=MESH,
        )

    def id_copy(k, end):
        return pltpu.make_async_remote_copy(
            src_ref=ids_ref, dst_ref=ids.at[k // per, end],
            send_sem=i_send.at[k], recv_sem=i_recv.at[k],
            device_id={"sp": flip(s, k, sp)}, device_id_type=MESH,
        )

    def result_copy(k):
        target = flip(s, k, sp)
        return pltpu.make_async_remote_copy(
            src_ref=res.at[k // per, pl.ds(pl.multiple_of((target % per) * tokens, tokens), tokens)],
            dst_ref=ret.at[k],
            send_sem=r_send.at[k], recv_sem=r_recv.at[k],
            device_id={"sp": target}, device_id_type=MESH,
        )

    for step in range(1, planes):
        mix_copy(mixing_ref, d, across(step), m_send.at[step]).start()
    mix_copy(mixing_ref, d, partner, m_send.at[0]).start()

    def send_one(k, carry):
        id_copy(k, half).start()
        value_copy(k, half).start()
        return carry

    lax.fori_loop(1, sp, send_one, 0)

    own = pltpu.make_async_copy(mixing_ref, chunk(d), own_sem)
    own.start()
    vals[0, pl.ds(pl.multiple_of(half * tokens, tokens), tokens), :] = value_ref[
        :, pl.ds(pl.multiple_of(s * HEAD_DIM, HEAD_DIM), HEAD_DIM)
    ]
    ids[0, half] = ids_ref[...]
    bias_col[...] = to_column(bias_ref[...].astype(jnp.float32))

    for step in range(1, planes):
        origin = across(planes - step)
        mix_copy(mixing_ref, origin, partner, m_send.at[0]).wait_recv()
        mix_copy(chunk(origin), origin, partner, m_fwd.at[step]).start()
    mix_copy(mixing_ref, partner, partner, m_send.at[0]).wait_recv()
    for step in range(1, planes):
        origin = across(planes - step)
        there = origin + 1 - 2 * (origin % CORES)
        mix_copy(mixing_ref, there, partner, m_send.at[0]).wait_recv()
    own.wait()

    gain = gain_ref[...].astype(jnp.float32)

    def one_block(j, carry):
        for i in range(per):
            k = j * per + i

            @pl.when(k > 0)
            def _():
                source_half = flip(s, k, sp) % per
                id_copy(k, source_half).wait_recv()
                value_copy(k, source_half).wait_recv()

        for at in range(0, block_len, ROW_STEP):
            act = gelu(vals[j, at : at + ROW_STEP, :].astype(jnp.float32))
            mean = jnp.mean(act * act, axis=-1, keepdims=True)
            normed[at : at + ROW_STEP, :] = (act * lax.rsqrt(mean + epsilon) * gain).astype(jnp.bfloat16)
        row = jnp.concatenate([ids[j, i] for i in range(per)], axis=1).astype(jnp.float32)
        ids_col[...] = to_column(row).astype(jnp.bfloat16)
        row_b = row.astype(jnp.bfloat16)
        right = normed[...]
        zero = jnp.zeros((), jnp.bfloat16)
        for at in range(0, block_len, ROW_STEP):
            col = ids_col[at : at + ROW_STEP, :]
            pieces = []
            for c in range(0, block_len, LANES):
                same = col == row_b[:, c : c + LANES]
                pieces.append(jnp.where(same, mix[at : at + ROW_STEP, c : c + LANES], zero))
            summed = jnp.dot(jnp.concatenate(pieces, axis=1), right, preferred_element_type=jnp.float32)
            res[j, at : at + ROW_STEP, :] = (summed + bias_col[at : at + ROW_STEP, :]).astype(jnp.bfloat16)
        for i in range(per):
            k = j * per + i

            @pl.when(k > 0)
            def _():
                result_copy(k).start()

        return carry

    lax.fori_loop(0, blocks, one_block, 0)
    ret[0] = res[0, pl.ds(pl.multiple_of(half * tokens, tokens), tokens), :]

    def finish(k, carry):
        @pl.when(k > 0)
        def _():
            result_copy(k).wait_recv()

        lanes = pl.ds(pl.multiple_of(flip(s, k, sp) * HEAD_DIM, HEAD_DIM), HEAD_DIM)
        for at in range(0, tokens, ROW_STEP):
            gate = gelu(gate_ref[at : at + ROW_STEP, lanes].astype(jnp.float32))
            got = ret[k, at : at + ROW_STEP, :].astype(jnp.float32)
            out_ref[at : at + ROW_STEP, lanes] = (gate * got).astype(jnp.bfloat16)
        return carry

    lax.fori_loop(0, sp, finish, 0)

    def drain(k, carry):
        id_copy(k, half).wait_send()
        value_copy(k, half).wait_send()
        result_copy(k).wait_send()
        return carry

    lax.fori_loop(1, sp, drain, 0)
    mix_copy(mixing_ref, d, partner, m_send.at[0]).wait_send()
    for step in range(1, planes):
        mix_copy(mixing_ref, d, across(step), m_send.at[step]).wait_send()
        origin = across(planes - step)
        mix_copy(chunk(origin), origin, partner, m_fwd.at[step]).wait_send()


def per_device(gate_in, value_in, segments, value_gain, mixing, mixing_bias):
    sp, dp = lax.axis_size("sp"), lax.axis_size("dp")
    sequences, tokens, width = value_in.shape
    heads_here, rows, block_len = mixing.shape
    assert sequences == 1 and heads_here == 1
    per = block_len // tokens
    blocks = sp // per
    bf16, f32 = jnp.bfloat16, jnp.float32
    dma = pltpu.SemaphoreType.DMA
    vmem, anywhere = pl.BlockSpec(memory_space=pltpu.VMEM), pl.BlockSpec(memory_space=pl.ANY)
    out = pl.pallas_call(
        functools.partial(kernel, sp, dp),
        out_shape=jax.ShapeDtypeStruct((tokens, width), bf16),
        in_specs=[vmem, vmem, vmem, anywhere, vmem, vmem],
        out_specs=vmem,
        scratch_shapes=[
            pltpu.VMEM((blocks, block_len, HEAD_DIM), bf16),
            pltpu.VMEM((blocks, per, 1, tokens), jnp.int32),
            pltpu.VMEM((block_len, block_len), bf16),
            pltpu.VMEM((blocks, block_len, HEAD_DIM), bf16),
            pltpu.VMEM((sp, tokens, HEAD_DIM), bf16),
            pltpu.VMEM((block_len, LANES), f32),
            pltpu.VMEM((block_len, HEAD_DIM), bf16),
            pltpu.VMEM((block_len, LANES), bf16),
            dma((sp,)), dma((sp,)), dma((sp,)), dma((sp,)), dma((sp,)), dma((sp,)),
            dma((dp // CORES,)), dma((dp,)), dma((dp // CORES,)), dma,
        ],
        compiler_params=pltpu.CompilerParams(
            collective_id=0, has_side_effects=True, vmem_limit_bytes=60 * 1024 * 1024
        ),
    )(
        value_in.reshape(tokens, width),
        segments,
        value_gain.reshape(1, HEAD_DIM),
        mixing.reshape(rows, block_len),
        mixing_bias,
        gate_in.reshape(tokens, width),
    )
    return out.reshape(sequences, tokens, width)


def solution(mesh):
    return jax.shard_map(
        per_device,
        mesh=mesh,
        in_specs=(
            P("dp", "sp", None),
            P("dp", "sp", None),
            P("dp", "sp"),
            P("sp"),
            P("sp", "dp", None),
            P("sp", None),
        ),
        out_specs=P("dp", "sp", None),
        check_vma=False,
    )
```

time: 163 us -> 55.8 us (0.34)
  the two profiles are of different devices: /device:TPU:0 before, /device:TPU:22 now
where the time goes in v1:
time: 55.8 us; the launch traced here: 55.6 us
  Pallas kernels  53.3 us (96%)
  local copies, waits for them, and re-layouts  2.26 us (4%)
    pallas_call x1, Pallas kernels, per_device(): pl.pallas_call(functools.partial(kernel, sp, dp), out_shape=jax.ShapeDtyp...  53.3 us
    unnamed x1, local copies, waits for them, and re-layouts  2.26 us

profile of v1, /device:TPU:22, one launch (start us, length us, event | category | flops | bytes accessed | tf_op | source)
XLA Modules:
  0.0 55.6 jit_solution(2860967244278898056)
XLA Ops:
  0.0 53.3 %shard_map.64 = bf16[512,1024]{1,0:T(8,128)(2,1)} custom-call(bf16[512,1024]{1,0:T(8,128)(2,1)} %bitcast.6, s32[1,512]{1,0:T(1,128)} %ids_ref.1, bf16[1,128]{1,0:T(2,128)(2,1)} %bitcast.9, bf16[256,1024]{1,0:T(8,128)(2,1)} %bitcast.8, bf16[1,1024]{1,0:T(2,128)(2,1)} %bias_ref.1, bf16[512,1024]{1,0:T(8,128)(2,1)} %bitcast.7), custom_call_target="tpu_custom_call" | custom-call | tf_op jit(solution)/shard_map/pallas_call | solution.py:209
  53.3 2.3 %copy.8 = bf16[1,512,1024]{2,1,0:T(8,128)(2,1)} copy(bf16[1,512,1024]{2,1,0:T(8,128)(2,1)} %bitcast.5) | data formatting | bytes 2097152

commit v2 on v1

--- a/solution.py
+++ b/solution.py
@@ -11,6 +11,7 @@
 CORES = 2
 LANES = 128
 ROW_STEP = 256
+PARTS = 4
 MESH = pl.DeviceIdType.MESH
 
 epsilon = 1e-06
@@ -38,14 +39,16 @@
 
 def kernel(
     sp, dp, value_ref, ids_ref, gain_ref, mixing_ref, bias_ref, gate_ref, out_ref,
-    vals, ids, mix, res, ret, bias_col, normed, ids_col,
+    vals, ids, mix, res, ret, bias_col, normed, ids_col, extras, extras_in,
     v_send, v_recv, i_send, i_recv, r_send, r_recv, m_send, m_recv, m_fwd, own_sem,
+    e_send, e_recv, far_send, far_recv, across_send, core_send, fwd_send,
 ):
     s, d = lax.axis_index("sp"), lax.axis_index("dp")
     tokens = value_ref.shape[0]
-    block_len = mix.shape[0]
+    block_len = mix.shape[1]
     per = block_len // tokens
-    blocks = sp // per
+    near = sp // 2
+    blocks = near // per
     rows = mixing_ref.shape[0]
     planes = dp // CORES
     half = s % per
@@ -55,16 +58,18 @@
     def across(step):
         return ((plane + step) % planes) * CORES + core
 
+    extras[:, :block_len] = bias_ref[...].astype(jnp.float32)
+    extras[:, block_len:] = gain_ref[...].astype(jnp.float32)
     barrier = pltpu.get_barrier_semaphore()
-    for k in range(1, sp):
+    for k in range(1, near + 1):
         pl.semaphore_signal(barrier, inc=1, device_id={"sp": flip(s, k, sp)}, device_id_type=MESH)
     pl.semaphore_signal(barrier, inc=1, device_id={"dp": partner}, device_id_type=MESH)
     for step in range(1, planes):
         pl.semaphore_signal(barrier, inc=1, device_id={"dp": across(step)}, device_id_type=MESH)
-    pl.semaphore_wait(barrier, sp - 1 + planes)
+    pl.semaphore_wait(barrier, near + planes)
 
     def chunk(of):
-        return mix.at[pl.ds(pl.multiple_of(of * rows, rows), rows)]
+        return mix.at[0, pl.ds(pl.multiple_of(of * rows, rows), rows)]
 
     def mix_copy(src, origin, target, sem):
         return pltpu.make_async_remote_copy(
@@ -72,10 +77,46 @@
             device_id={"dp": target}, device_id_type=MESH,
         )
 
+    part = rows // PARTS
+
+    def far_part(origin, q):
+        return mix.at[1, pl.ds(pl.multiple_of(origin * rows + q * part, part), part)]
+
+    def far_copy(src, origin, q, where, sem):
+        return pltpu.make_async_remote_copy(
+            src_ref=src, dst_ref=far_part(origin, q), send_sem=sem,
+            recv_sem=far_recv.at[origin * PARTS + q], device_id=where, device_id_type=MESH,
+        )
+
+    def from_far(q):
+        return far_copy(
+            mixing_ref.at[pl.ds(q * part, part)], d, q, {"sp": flip(s, near, sp)}, far_send.at[q]
+        )
+
+    def to_plane(step, q):
+        return far_copy(
+            far_part(d, q), d, q, {"dp": across(step)}, across_send.at[step * PARTS + q]
+        )
+
+    def to_core(q):
+        return far_copy(far_part(d, q), d, q, {"dp": partner}, core_send.at[q])
+
+    def pass_on(step, q):
+        origin = across(planes - step)
+        return far_copy(
+            far_part(origin, q), origin, q, {"dp": partner}, fwd_send.at[step * PARTS + q]
+        )
+
+    def extras_copy():
+        return pltpu.make_async_remote_copy(
+            src_ref=extras, dst_ref=extras_in, send_sem=e_send, recv_sem=e_recv,
+            device_id={"sp": flip(s, near, sp)}, device_id_type=MESH,
+        )
+
     def value_copy(k, end):
-        target = flip(s, k, sp)
-        return pltpu.make_async_remote_copy(
-            src_ref=value_ref.at[:, pl.ds(pl.multiple_of(target * HEAD_DIM, HEAD_DIM), HEAD_DIM)],
+        target, head = flip(s, k % near, sp), flip(s, k, sp)
+        return pltpu.make_async_remote_copy(
+            src_ref=value_ref.at[:, pl.ds(pl.multiple_of(head * HEAD_DIM, HEAD_DIM), HEAD_DIM)],
             dst_ref=vals.at[k // per, pl.ds(pl.multiple_of(end * tokens, tokens), tokens)],
             send_sem=v_send.at[k], recv_sem=v_recv.at[k],
             device_id={"sp": target}, device_id_type=MESH,
@@ -89,7 +130,7 @@
         )
 
     def result_copy(k):
-        target = flip(s, k, sp)
+        target = flip(s, k % near, sp)
         return pltpu.make_async_remote_copy(
             src_ref=res.at[k // per, pl.ds(pl.multiple_of((target % per) * tokens, tokens), tokens)],
             dst_ref=ret.at[k],
@@ -106,15 +147,24 @@
         value_copy(k, half).start()
         return carry
 
-    lax.fori_loop(1, sp, send_one, 0)
+    def send_more(k, carry):
+        value_copy(k, half).start()
+        return carry
+
+    extras_copy().start()
+    lax.fori_loop(1, near, send_one, 0)
+    for q in range(PARTS):
+        from_far(q).start()
+    lax.fori_loop(near + 1, sp, send_more, 0)
 
     own = pltpu.make_async_copy(mixing_ref, chunk(d), own_sem)
     own.start()
-    vals[0, pl.ds(pl.multiple_of(half * tokens, tokens), tokens), :] = value_ref[
-        :, pl.ds(pl.multiple_of(s * HEAD_DIM, HEAD_DIM), HEAD_DIM)
-    ]
+    for k in (0, near):
+        vals[k // per, pl.ds(pl.multiple_of(half * tokens, tokens), tokens), :] = value_ref[
+            :, pl.ds(pl.multiple_of(flip(s, k, sp) * HEAD_DIM, HEAD_DIM), HEAD_DIM)
+        ]
     ids[0, half] = ids_ref[...]
-    bias_col[...] = to_column(bias_ref[...].astype(jnp.float32))
+    bias_col[0] = to_column(extras[:, :block_len])
 
     for step in range(1, planes):
         origin = across(planes - step)
@@ -127,20 +177,21 @@
         mix_copy(mixing_ref, there, partner, m_send.at[0]).wait_recv()
     own.wait()
 
-    gain = gain_ref[...].astype(jnp.float32)
-
-    def one_block(j, carry):
+    def one_block(which, j):
+        gain = (extras, extras_in)[which][:, block_len:]
+        at_block = which * blocks + j
         for i in range(per):
             k = j * per + i
 
             @pl.when(k > 0)
             def _():
                 source_half = flip(s, k, sp) % per
-                id_copy(k, source_half).wait_recv()
-                value_copy(k, source_half).wait_recv()
+                if which == 0:
+                    id_copy(k, source_half).wait_recv()
+                value_copy(k + which * near, source_half).wait_recv()
 
         for at in range(0, block_len, ROW_STEP):
-            act = gelu(vals[j, at : at + ROW_STEP, :].astype(jnp.float32))
+            act = gelu(vals[at_block, at : at + ROW_STEP, :].astype(jnp.float32))
             mean = jnp.mean(act * act, axis=-1, keepdims=True)
             normed[at : at + ROW_STEP, :] = (act * lax.rsqrt(mean + epsilon) * gain).astype(jnp.bfloat16)
         row = jnp.concatenate([ids[j, i] for i in range(per)], axis=1).astype(jnp.float32)
@@ -153,23 +204,58 @@
             pieces = []
             for c in range(0, block_len, LANES):
                 same = col == row_b[:, c : c + LANES]
-                pieces.append(jnp.where(same, mix[at : at + ROW_STEP, c : c + LANES], zero))
+                pieces.append(jnp.where(same, mix[which, at : at + ROW_STEP, c : c + LANES], zero))
             summed = jnp.dot(jnp.concatenate(pieces, axis=1), right, preferred_element_type=jnp.float32)
-            res[j, at : at + ROW_STEP, :] = (summed + bias_col[at : at + ROW_STEP, :]).astype(jnp.bfloat16)
+            res[at_block, at : at + ROW_STEP, :] = (summed + bias_col[which, at : at + ROW_STEP, :]).astype(jnp.bfloat16)
         for i in range(per):
             k = j * per + i
 
             @pl.when(k > 0)
             def _():
-                result_copy(k).start()
-
-        return carry
-
-    lax.fori_loop(0, blocks, one_block, 0)
-    ret[0] = res[0, pl.ds(pl.multiple_of(half * tokens, tokens), tokens), :]
+                result_copy(k + which * near).start()
+
+    def relay(q):
+        from_far(q).wait_recv()
+        for step in range(1, planes):
+            to_plane(step, q).start()
+        to_core(q).start()
+
+    def some_blocks(first, last):
+        def body(j, carry):
+            one_block(0, j)
+            return carry
+
+        lax.fori_loop(first, last, body, 0)
+
+    relay(0)
+    relay(1)
+    some_blocks(0, blocks // 2)
+    relay(2)
+    some_blocks(blocks // 2, blocks)
+    relay(3)
+    extras_copy().wait_recv()
+    bias_col[1] = to_column(extras_in[:, :block_len])
+    for q in range(PARTS):
+        for step in range(1, planes):
+            pass_on(step, q).wait_recv()
+            pass_on(step, q).start()
+    for q in range(PARTS):
+        far_copy(far_part(d, q), partner, q, {"dp": partner}, core_send.at[q]).wait_recv()
+        for step in range(1, planes):
+            origin = across(planes - step)
+            there = origin + 1 - 2 * (origin % CORES)
+            far_copy(far_part(d, q), there, q, {"dp": partner}, core_send.at[q]).wait_recv()
+
+    def far_block(n, carry):
+        one_block(1, blocks - 1 - n)
+        return carry
+
+    lax.fori_loop(0, blocks, far_block, 0)
+    for k in (0, near):
+        ret[k] = res[k // per, pl.ds(pl.multiple_of(half * tokens, tokens), tokens), :]
 
     def finish(k, carry):
-        @pl.when(k > 0)
+        @pl.when(k % near > 0)
         def _():
             result_copy(k).wait_recv()
 
@@ -184,11 +270,19 @@
 
     def drain(k, carry):
         id_copy(k, half).wait_send()
-        value_copy(k, half).wait_send()
-        result_copy(k).wait_send()
-        return carry
-
-    lax.fori_loop(1, sp, drain, 0)
+        for n in (k, k + near):
+            value_copy(n, half).wait_send()
+            result_copy(n).wait_send()
+        return carry
+
+    lax.fori_loop(1, near, drain, 0)
+    extras_copy().wait_send()
+    for q in range(PARTS):
+        from_far(q).wait_send()
+        to_core(q).wait_send()
+        for step in range(1, planes):
+            to_plane(step, q).wait_send()
+            pass_on(step, q).wait_send()
     mix_copy(mixing_ref, d, partner, m_send.at[0]).wait_send()
     for step in range(1, planes):
         mix_copy(mixing_ref, d, across(step), m_send.at[step]).wait_send()
@@ -202,7 +296,8 @@
     heads_here, rows, block_len = mixing.shape
     assert sequences == 1 and heads_here == 1
     per = block_len // tokens
-    blocks = sp // per
+    near = sp // 2
+    blocks = near // per
     bf16, f32 = jnp.bfloat16, jnp.float32
     dma = pltpu.SemaphoreType.DMA
     vmem, anywhere = pl.BlockSpec(memory_space=pltpu.VMEM), pl.BlockSpec(memory_space=pl.ANY)
@@ -212,16 +307,20 @@
         in_specs=[vmem, vmem, vmem, anywhere, vmem, vmem],
         out_specs=vmem,
         scratch_shapes=[
-            pltpu.VMEM((blocks, block_len, HEAD_DIM), bf16),
+            pltpu.VMEM((2 * blocks, block_len, HEAD_DIM), bf16),
             pltpu.VMEM((blocks, per, 1, tokens), jnp.int32),
-            pltpu.VMEM((block_len, block_len), bf16),
-            pltpu.VMEM((blocks, block_len, HEAD_DIM), bf16),
+            pltpu.VMEM((2, block_len, block_len), bf16),
+            pltpu.VMEM((2 * blocks, block_len, HEAD_DIM), bf16),
             pltpu.VMEM((sp, tokens, HEAD_DIM), bf16),
-            pltpu.VMEM((block_len, LANES), f32),
+            pltpu.VMEM((2, block_len, LANES), f32),
             pltpu.VMEM((block_len, HEAD_DIM), bf16),
             pltpu.VMEM((block_len, LANES), bf16),
+            pltpu.VMEM((1, block_len + HEAD_DIM), f32),
+            pltpu.VMEM((1, block_len + HEAD_DIM), f32),
             dma((sp,)), dma((sp,)), dma((sp,)), dma((sp,)), dma((sp,)), dma((sp,)),
             dma((dp // CORES,)), dma((dp,)), dma((dp // CORES,)), dma,
+            dma, dma, dma((PARTS,)), dma((dp * PARTS,)), dma((dp // CORES * PARTS,)),
+            dma((PARTS,)), dma((dp // CORES * PARTS,)),
         ],
         compiler_params=pltpu.CompilerParams(
             collective_id=0, has_side_effects=True, vmem_limit_bytes=60 * 1024 * 1024

time: 55.8 us -> 50.4 us (0.903)
  the two profiles are of different devices: /device:TPU:22 before, /device:TPU:0 now
where the time goes in v2:
time: 50.4 us; the launch traced here: 50.2 us
  Pallas kernels  47.9 us (95%)
  local copies, waits for them, and re-layouts  2.26 us (4%)
    pallas_call x1, Pallas kernels, per_device(): pl.pallas_call(functools.partial(kernel, sp, dp), out_shape=jax.ShapeDtyp...  47.9 us
    unnamed x1, local copies, waits for them, and re-layouts  2.26 us

profile of v2, /device:TPU:0, one launch (start us, length us, event | category | flops | bytes accessed | tf_op | source)
XLA Modules:
  0.0 50.2 jit_solution(1900856004259756125)
XLA Ops:
  0.0 47.9 %shard_map.64 = bf16[512,1024]{1,0:T(8,128)(2,1)} custom-call(bf16[512,1024]{1,0:T(8,128)(2,1)} %bitcast.6, s32[1,512]{1,0:T(1,128)} %ids_ref.1, bf16[1,128]{1,0:T(2,128)(2,1)} %bitcast.9, bf16[256,1024]{1,0:T(8,128)(2,1)} %bitcast.8, bf16[1,1024]{1,0:T(2,128)(2,1)} %bias_ref.1, bf16[512,1024]{1,0:T(8,128)(2,1)} %bitcast.7), custom_call_target="tpu_custom_call" | custom-call | tf_op jit(solution)/shard_map/pallas_call | solution.py:304
  47.9 2.3 %copy.8 = bf16[1,512,1024]{2,1,0:T(8,128)(2,1)} copy(bf16[1,512,1024]{2,1,0:T(8,128)(2,1)} %bitcast.5) | data formatting | bytes 2097152

commit v3 on v2

--- a/solution.py
+++ b/solution.py
@@ -195,12 +195,12 @@
             mean = jnp.mean(act * act, axis=-1, keepdims=True)
             normed[at : at + ROW_STEP, :] = (act * lax.rsqrt(mean + epsilon) * gain).astype(jnp.bfloat16)
         row = jnp.concatenate([ids[j, i] for i in range(per)], axis=1).astype(jnp.float32)
-        ids_col[...] = to_column(row).astype(jnp.bfloat16)
+        ids_col[j] = to_column(row).astype(jnp.bfloat16)
         row_b = row.astype(jnp.bfloat16)
         right = normed[...]
         zero = jnp.zeros((), jnp.bfloat16)
         for at in range(0, block_len, ROW_STEP):
-            col = ids_col[at : at + ROW_STEP, :]
+            col = ids_col[j, at : at + ROW_STEP, :]
             pieces = []
             for c in range(0, block_len, LANES):
                 same = col == row_b[:, c : c + LANES]
@@ -235,19 +235,74 @@
     relay(3)
     extras_copy().wait_recv()
     bias_col[1] = to_column(extras_in[:, :block_len])
-    for q in range(PARTS):
+    def relay_on(q):
         for step in range(1, planes):
             pass_on(step, q).wait_recv()
             pass_on(step, q).start()
-    for q in range(PARTS):
-        far_copy(far_part(d, q), partner, q, {"dp": partner}, core_send.at[q]).wait_recv()
-        for step in range(1, planes):
-            origin = across(planes - step)
-            there = origin + 1 - 2 * (origin % CORES)
-            far_copy(far_part(d, q), there, q, {"dp": partner}, core_send.at[q]).wait_recv()
+
+    def far_ready(j, carry):
+        gain = extras_in[:, block_len:]
+        for i in range(per):
+            k = j * per + i
+
+            @pl.when(k > 0)
+            def _():
+                value_copy(k + near, flip(s, k, sp) % per).wait_recv()
+
+        for at in range(0, block_len, ROW_STEP):
+            act = gelu(vals[blocks + j, at : at + ROW_STEP, :].astype(jnp.float32))
+            mean = jnp.mean(act * act, axis=-1, keepdims=True)
+            vals[blocks + j, at : at + ROW_STEP, :] = (
+                act * lax.rsqrt(mean + epsilon) * gain
+            ).astype(jnp.bfloat16)
+        return carry
+
+    def far_rows(origin):
+        span = pl.ds(pl.multiple_of(origin * rows, rows), rows)
+
+        def body(j, carry):
+            row = jnp.concatenate([ids[j, i] for i in range(per)], axis=1)
+            row_b = row.astype(jnp.float32).astype(jnp.bfloat16)
+            col = ids_col[j, span, :]
+            pieces = []
+            for c in range(0, block_len, LANES):
+                same = col == row_b[:, c : c + LANES]
+                pieces.append(jnp.where(same, mix[1, span, c : c + LANES], jnp.zeros((), jnp.bfloat16)))
+            summed = jnp.dot(
+                jnp.concatenate(pieces, axis=1), vals[blocks + j], preferred_element_type=jnp.float32
+            )
+            res[blocks + j, span, :] = (summed + bias_col[1, span, :]).astype(jnp.bfloat16)
+            return carry
+
+        lax.fori_loop(0, blocks, body, 0)
+
+    def arrived(origin):
+        for q in range(PARTS):
+            far_copy(far_part(d, q), origin, q, {"dp": partner}, core_send.at[q]).wait_recv()
+
+    for q in range(PARTS - 1):
+        relay_on(q)
+    lax.fori_loop(0, blocks, far_ready, 0)
+    far_rows(d)
+    relay_on(PARTS - 1)
+    arrived(partner)
+    far_rows(partner)
+    for step in range(1, planes):
+        origin = across(planes - step)
+        far_rows(origin)
+        there = origin + 1 - 2 * (origin % CORES)
+        arrived(there)
+        far_rows(there)
 
     def far_block(n, carry):
-        one_block(1, blocks - 1 - n)
+        j = blocks - 1 - n
+        for i in range(per):
+            k = j * per + i
+
+            @pl.when(k > 0)
+            def _():
+                result_copy(k + near).start()
+
         return carry
 
     lax.fori_loop(0, blocks, far_block, 0)
@@ -314,7 +369,7 @@
             pltpu.VMEM((sp, tokens, HEAD_DIM), bf16),
             pltpu.VMEM((2, block_len, LANES), f32),
             pltpu.VMEM((block_len, HEAD_DIM), bf16),
-            pltpu.VMEM((block_len, LANES), bf16),
+            pltpu.VMEM((blocks, block_len, LANES), bf16),
             pltpu.VMEM((1, block_len + HEAD_DIM), f32),
             pltpu.VMEM((1, block_len + HEAD_DIM), f32),
             dma((sp,)), dma((sp,)), dma((sp,)), dma((sp,)), dma((sp,)), dma((sp,)),

time: 50.4 us -> 50.9 us (level)
    pallas_call x1, Pallas kernels: 47.9 us -> 48.4 us  [per_device(): pl.pallas_call(functools.partial(kernel, sp, dp), out_shape=jax.ShapeDtyp...]
where the time goes in v3:
time: 50.9 us; the launch traced here: 50.7 us
  Pallas kernels  48.4 us (95%)
  local copies, waits for them, and re-layouts  2.26 us (4%)
    pallas_call x1, Pallas kernels, per_device(): pl.pallas_call(functools.partial(kernel, sp, dp), out_shape=jax.ShapeDtyp...  48.4 us
    unnamed x1, local copies, waits for them, and re-layouts  2.26 us

profile of v3, /device:TPU:0, one launch (start us, length us, event | category | flops | bytes accessed | tf_op | source)
XLA Modules:
  0.0 50.7 jit_solution(14842467254035620614)
XLA Ops:
  0.0 48.4 %shard_map.64 = bf16[512,1024]{1,0:T(8,128)(2,1)} custom-call(bf16[512,1024]{1,0:T(8,128)(2,1)} %bitcast.6, s32[1,512]{1,0:T(1,128)} %ids_ref.1, bf16[1,128]{1,0:T(2,128)(2,1)} %bitcast.9, bf16[256,1024]{1,0:T(8,128)(2,1)} %bitcast.8, bf16[1,1024]{1,0:T(2,128)(2,1)} %bias_ref.1, bf16[512,1024]{1,0:T(8,128)(2,1)} %bitcast.7), custom_call_target="tpu_custom_call" | custom-call | tf_op jit(solution)/shard_map/pallas_call | solution.py:359
  48.4 2.3 %copy.8 = bf16[1,512,1024]{2,1,0:T(8,128)(2,1)} copy(bf16[1,512,1024]{2,1,0:T(8,128)(2,1)} %bitcast.5) | data formatting | bytes 2097152
